TPU v7x, 32 devices: a whole 2x2x4 slice. The times are simulated.
32 devices in a mesh: rep: 2 (over y), fs: 4 (over z), tp: 4 (over x, core).
Axes of the slice: x: 2, y: 2, z: 4, core: 2. Of those that a mesh axis runs over, the one named last changes fastest.
Arguments:
- stream: bfloat16 [2048, 2048], P(('rep', 'fs')), may hold values from -6 to 6
- gain_mix: float32 [2048], replicated, may hold values from 0.1 to 1.9
- w_query: float32 [2048, 2048], P('fs', 'tp'), may hold values from -0.125 to 0.125
- scale_query: float32 [2048], P('tp'), may hold values from 0.5 to 2
- w_key: float32 [2048, 2048], P('fs', 'tp'), may hold values from -0.125 to 0.125
- scale_key: float32 [2048], P('tp'), may hold values from 0.5 to 2
- w_value: float32 [2048, 2048], P('fs', 'tp'), may hold values from -0.125 to 0.125
- scale_value: float32 [2048], P('tp'), may hold values from 0.5 to 2
- gain_ffn: float32 [2048], replicated, may hold values from 0.1 to 1.9
- w_gate: float32 [2048, 2816], P('fs', 'tp'), may hold values from -0.125 to 0.125
- scale_gate: float32 [2816], P('tp'), may hold values from 0.5 to 2
- w_up: float32 [2048, 2816], P('fs', 'tp'), may hold values from -0.125 to 0.125
- scale_up: float32 [2816], P('tp'), may hold values from 0.5 to 2
- w_down: float32 [2048, 2816], P('fs', 'tp'), may hold values from -0.109375 to 0.109375
- scale_down: float32 [2048], P('fs'), may hold values from 0.5 to 2
Outputs:
- layer_out: bfloat16 [2048, 2048], P(('rep', 'fs', 'tp'))
All inputs are finite; a program needn't handle non-finite values.
Results may differ from a plain program's by a relative error of at most 0.015.
Values may be sent and summed in bfloat16 or wider, within the bound.
A program may use at most 64 MiB of HBM per device.

v0:
```python
import jax
import jax.numpy as jnp
from jax import lax
from jax.sharding import PartitionSpec as P

DK = 256
DV = 256
LEN = 128
BLK = 64


EPS = 1e-06
THETA = 10000.0
HIGH = lax.Precision.HIGHEST


def rms_scale(values):
    return lax.rsqrt(jnp.mean(values * values, axis=-1, keepdims=True) + EPS)


def head_scale(values):
    return 1.0 / jnp.maximum(jnp.sqrt(jnp.mean(values * values, axis=-1, keepdims=True)), 1.0)


def rotate(heads_data, positions):
    half = heads_data.shape[-1] // 2
    frequency = THETA ** (-(jnp.arange(half, dtype=jnp.float32) / half))
    angle = positions.astype(jnp.float32)[:, None, None] * frequency
    cosine = jnp.cos(angle)
    sine = jnp.sin(angle)
    first = heads_data[..., :half]
    second = heads_data[..., half:]
    return jnp.concatenate(
        [first * cosine - second * sine, second * cosine + first * sine], axis=-1
    )


def retention_blocks(queries, keys, values, log_decay):
    total_rows, heads, key_width = queries.shape
    value_width = values.shape[-1]
    queries = queries.reshape((-1, LEN // BLK, BLK, heads, key_width))
    keys = keys.reshape((-1, LEN // BLK, BLK, heads, key_width))
    values = values.reshape((-1, LEN // BLK, BLK, heads, value_width))
    offsets = jnp.arange(BLK, dtype=jnp.float32)
    distance = offsets[:, None] - offsets[None, :]
    decay_mask = jnp.where(
        distance >= 0, jnp.exp(log_decay[:, None, None] * jnp.maximum(distance, 0.0)), 0.0
    )
    scores = jnp.einsum("snihd,snjhd->snhij", queries, keys, precision=HIGH) * decay_mask
    inner = jnp.einsum("snhij,snjhe->snihe", scores, values, precision=HIGH)
    query_decay = jnp.exp(log_decay[None, :] * (offsets[:, None] + 1.0))[:, :, None]
    key_decay = jnp.exp(log_decay[None, :] * (BLK - 1.0 - offsets[:, None]))[:, :, None]
    block_decay = jnp.exp(log_decay * BLK)[None, :, None, None]

    def advance(state, inputs):
        block_query, block_key, block_value = inputs
        carried = jnp.einsum("sihd,shde->sihe", block_query, state, precision=HIGH)
        state = state * block_decay + jnp.einsum(
            "sjhd,sjhe->shde", block_key, block_value, precision=HIGH
        )
        return (state, carried)

    moved = (
        jnp.moveaxis(queries * query_decay, 1, 0),
        jnp.moveaxis(keys * key_decay, 1, 0),
        jnp.moveaxis(values, 1, 0),
    )
    initial = jnp.zeros((queries.shape[0], heads, key_width, value_width), jnp.float32)
    _, carried = lax.scan(advance, initial, moved)
    return (inner + jnp.moveaxis(carried, 0, 1)).reshape(total_rows, heads, value_width)


def shards(
    stream,
    gain_mix,
    w_query,
    scale_query,
    w_key,
    scale_key,
    w_value,
    scale_value,
    gain_ffn,
    w_gate,
    scale_gate,
    w_up,
    scale_up,
    w_down,
    scale_down,
):
    group_rows = stream.shape[0]
    stream_f = stream.astype(jnp.float32)
    normed = (stream_f * rms_scale(stream_f) * gain_mix).astype(jnp.bfloat16)
    query_rounded = w_query.astype(jnp.bfloat16)
    key_rounded = w_key.astype(jnp.bfloat16)
    value_rounded = w_value.astype(jnp.bfloat16)
    gate_rounded = w_gate.astype(jnp.bfloat16)
    up_rounded = w_up.astype(jnp.bfloat16)
    down_rounded = w_down.astype(jnp.bfloat16)
    query_whole, key_whole, value_whole, gate_whole, up_whole, down_whole = (
        lax.all_gather(query_rounded, "fs", axis=0, tiled=True),
        lax.all_gather(key_rounded, "fs", axis=0, tiled=True),
        lax.all_gather(value_rounded, "fs", axis=0, tiled=True),
        lax.all_gather(gate_rounded, "fs", axis=0, tiled=True),
        lax.all_gather(up_rounded, "fs", axis=0, tiled=True),
        lax.all_gather(down_rounded, "fs", axis=0, tiled=True),
    )
    query_acc = jnp.dot(normed, query_whole, preferred_element_type=jnp.float32)
    key_acc = jnp.dot(normed, key_whole, preferred_element_type=jnp.float32)
    value_acc = jnp.dot(normed, value_whole, preferred_element_type=jnp.float32)
    query = (query_acc * scale_query).astype(jnp.bfloat16)
    key = (key_acc * scale_key).astype(jnp.bfloat16)
    value = (value_acc * scale_value).astype(jnp.bfloat16)
    local_heads = query.shape[1] // DK
    positions = jnp.arange(group_rows, dtype=jnp.int32) % LEN
    queries = rotate(query.astype(jnp.float32).reshape(group_rows, local_heads, DK), positions)
    keys = rotate(key.astype(jnp.float32).reshape(group_rows, local_heads, DK), positions) * DK ** (
        -0.5
    )
    values = value.astype(jnp.float32).reshape(group_rows, local_heads, DV)
    head_ids = (
        lax.axis_index("tp") * local_heads + jnp.arange(local_heads, dtype=jnp.int32)
    ).astype(jnp.float32)
    log_decay = jnp.log(1.0 - jnp.power(2.0, -5.0 - head_ids))
    down_scale = lax.all_gather(scale_down, "fs", axis=0, tiled=True)
    retained = retention_blocks(queries, keys, values, log_decay)
    mixed = (
        (retained * head_scale(retained)).astype(jnp.bfloat16).reshape(group_rows, local_heads * DV)
    )
    arrived = lax.all_to_all(mixed, "tp", split_axis=0, concat_axis=1, tiled=True)
    share = arrived.shape[0]
    own_rows = lax.dynamic_slice_in_dim(stream_f, lax.axis_index("tp") * share, share, 0)
    resid = own_rows + arrived.astype(jnp.float32)
    normed_ffn = (resid * rms_scale(resid) * gain_ffn).astype(jnp.bfloat16)
    piece = lax.all_gather(normed_ffn, "tp", axis=0, tiled=True)
    gate = jnp.dot(piece, gate_whole, preferred_element_type=jnp.float32) * scale_gate
    upward = jnp.dot(piece, up_whole, preferred_element_type=jnp.float32) * scale_up
    hidden = (jax.nn.silu(gate) * upward).astype(jnp.bfloat16)
    piece = hidden
    partial_sum = (
        lax.dot_general(
            piece, down_whole, (((1,), (1,)), ((), ())), preferred_element_type=jnp.float32
        )
        * down_scale
    )
    partial_sum = lax.optimization_barrier(partial_sum.astype(jnp.bfloat16))
    channel_out = lax.psum_scatter(
        partial_sum.astype(jnp.float32).astype(jnp.bfloat16), "tp", scatter_dimension=0, tiled=True
    ).astype(jnp.float32)
    return (resid + channel_out).astype(jnp.bfloat16)


def solution(mesh):
    placed = (
        P(("rep", "fs"), None),
        P(),
        P("fs", "tp"),
        P("tp"),
        P("fs", "tp"),
        P("tp"),
        P("fs", "tp"),
        P("tp"),
        P(),
        P("fs", "tp"),
        P("tp"),
        P("fs", "tp"),
        P("tp"),
        P("fs", "tp"),
        P("fs"),
    )
    return jax.shard_map(
        shards, mesh=mesh, in_specs=placed, out_specs=P(("rep", "fs", "tp"), None), check_vma=False
    )
```

profile of v0, /device:TPU:0, one launch (start us, length us, event | category | flops | bytes accessed | tf_op | source)
XLA Modules:
  0.0 384.9 jit_solution(17803356339925867683)
XLA Ops:
  6.5 2.2 convert_element_type.113
  8.9 0.9 convert_element_type.116
  9.8 0.9 convert_element_type.111
  10.8 1.0 convert_element_type.125
  13.2 44.2 %all-gather.11.cloned.1.call-done = bf16[2048,512]{1,0:T(8,128)(2,1)} async-done(((bf16[512,512]{1,0:T(8,128)(2,1)}), bf16[2048,512]{1,0:T(8,128)(2,1)}) %all-gather.11.cloned.1.call-update) | async-done | bytes 2097168 | tf_op jit(solution)/shard_map/all_gather | solution.py:100
  57.3 2.3 fusion.20
  60.0 43.4 %all-gather.13.cloned.1.call-done = bf16[2048,512]{1,0:T(8,128)(2,1)} async-done(((bf16[512,512]{1,0:T(8,128)(2,1)}), bf16[2048,512]{1,0:T(8,128)(2,1)}) %all-gather.13.cloned.1.call-update) | async-done | bytes 2097168 | tf_op jit(solution)/shard_map/all_gather | solution.py:101
  103.4 3.1 fusion.19
  106.5 1.4 reshape.295
  108.4 41.1 %all-gather.9.cloned.1.call-done = bf16[2048,512]{1,0:T(8,128)(2,1)} async-done(((bf16[512,512]{1,0:T(8,128)(2,1)}), bf16[2048,512]{1,0:T(8,128)(2,1)}) %all-gather.9.cloned.1.call-update) | async-done | bytes 2097168 | tf_op jit(solution)/shard_map/all_gather | solution.py:102
  149.5 3.0 fusion.16
  152.6 1.0 reshape_reshape.4
  153.7 1.3 convolution_multiply_fusion.6
  155.2 5.4 %while.13 = (s32[]{:T(128)}, f32[2,2,256,256]{3,2,1,0:T(8,128)S(1)}, f32[2,2,64,2,256]{4,2,3,0,1:T(8,128)}, f32[2,2,64,2,256]{4,2,3,0,1:T(8,128)S(1)}, f32[2,2,6...) while((s32[]{:T(128)}, ...), condition=%wide.region_2.3_spmd.clone, body=%wide.region_1.2_spmd.clone.sunk | while | flops 403701760 | bytes 4196980 | solution.py:69
  155.2 1.5 fusion.51
  156.7 1.2 convolution_add_fusion.2
  157.9 1.5 fusion.51
  159.4 1.2 convolution_add_fusion.2
  160.6 1.5 multiply_reduce_fusion.2
  164.6 3.4 all-to-all-start
  168.4 5.7 %all-to-all-done = bf16[4,64,512]{2,1,0:T(8,128)(2,1)S(1)} async-done(((bf16[4,64,512]{2,1,0:T(8,128)(2,1)}), bf16[4,64,512]{2,1,0:T(8,128)(2,1)S(1)}, u32[]{:S(2)}, u32[]{:S(2)}) %all-to-all-start) | async-done | bytes 262176 | tf_op jit(solution)/shard_map/all_to_all | solution.py:129
  175.2 2.4 convert_element_type.126
  177.7 0.9 convert_element_type.128
  178.7 12.6 %all-gather = f32[4,1,512]{2,1,0:T(1,128)S(1)} all-gather(f32[1,1,512]{2,1,0:T(1,128)S(1)} %bitcast.71), channel_id=1, replica_groups=mesh['rep'=2,'fs'=4,'tp'=4] {'fs'}, dimensions={0}, use_global_device_ids=true | all-gather | bytes 10240 | tf_op jit(solution)/shard_map/all_gather | solution.py:124
  191.3 17.6 %all-gather.17.cloned.1.call-done = bf16[2048,704]{0,1:T(8,128)(2,1)} async-done(((bf16[512,704]{0,1:T(8,128)(2,1)}), bf16[2048,704]{0,1:T(8,128)(2,1)}) %all-gather.17.cloned.1.call-update) | async-done | bytes 2883600 | tf_op jit(solution)/shard_map/all_gather | solution.py:103
  208.9 16.9 %all-gather.15.cloned.1.call-done = bf16[256,2048]{1,0:T(8,128)(2,1)} async-done(((bf16[64,2048]{1,0:T(8,128)(2,1)}), bf16[256,2048]{1,0:T(8,128)(2,1)}) %all-gather.15.cloned.1.call-update) | async-done | bytes 1048592 | tf_op jit(solution)/shard_map/all_gather | solution.py:134
  225.8 3.2 convolution_multiply_fusion.2
  228.9 57.4 %all-gather.19.cloned.1.call-done = bf16[2048,704]{0,1:T(8,128)(2,1)} async-done(((bf16[512,704]{0,1:T(8,128)(2,1)}), bf16[2048,704]{0,1:T(8,128)(2,1)}) %all-gather.19.cloned.1.call-update) | async-done | bytes 2883600 | tf_op jit(solution)/shard_map/all_gather | solution.py:104
  286.3 59.4 %all-gather.21.cloned.1.call-done = bf16[2048,704]{0,1:T(8,128)(2,1)} async-done(((bf16[512,704]{0,1:T(8,128)(2,1)}), bf16[2048,704]{0,1:T(8,128)(2,1)}) %all-gather.21.cloned.1.call-update) | async-done | bytes 2883600 | tf_op jit(solution)/shard_map/all_gather | solution.py:105
  345.7 7.0 %fusion.12 = bf16[256,2048]{1,0:T(8,128)(2,1)} fusion(bf16[2048,704]{0,1:T(8,128)(2,1)} %all-gather.21.cloned.1.call-done, f32[2048]{0:T(1024)S(1)} %bitcast.70, bf16[256,2048]{1,0:T(8,128)(2,1)S(1)} %copy-done.9, bf16[2048,704]{0,1:T(8,128)(2,1)} %all-gather.19.cloned.1.call-done, f32[256,704]{0,1:T(8,128)S(1)} %convolution_multiply_fusion.2, ...), kind=kOutput, calls=%fused_computation.17 | convolution fusion | flops 1478705152 | bytes 8596224 | tf_op jit(solution)/shard_map/dot_general | solution.py:140
  352.7 23.6 %reduce-scatter.2.cloned.1.call-done = bf16[64,2048]{1,0:T(8,128)(2,1)} async-done(((bf16[256,2048]{1,0:T(8,128)(2,1)}), bf16[64,2048]{1,0:T(8,128)(2,1)}) %reduce-scatter.2.cloned.1.call-update) | async-done | bytes 262160 | tf_op jit(solution)/shard_map/reduce_scatter | solution.py:146
  376.3 1.7 add_convert_fusion
  (83 shorter events, 6.7 us)
Async XLA Ops:
  6.5 2.3 copy-start.4
  6.5 3.3 copy-start.5
  6.5 50.8 %all-gather.11.cloned.1.call-start = ((), (), s32[]{:S(2)}) async-start(), calls=%async_computation.3 | async-start | bytes 2621440 | tf_op jit(solution)/shard_map/all_gather | solution.py:100
  8.8 2.0 copy-start.2
  8.8 94.6 %all-gather.13.cloned.1.call-start = ((), (), s32[]{:S(2)}) async-start(), calls=%async_computation.4 | async-start | bytes 2621440 | tf_op jit(solution)/shard_map/all_gather | solution.py:101
  9.8 139.7 %all-gather.9.cloned.1.call-start = ((), (), s32[]{:S(2)}) async-start(), calls=%async_computation.2 | async-start | bytes 2621440 | tf_op jit(solution)/shard_map/all_gather | solution.py:102
  10.7 1.5 copy-start
  10.7 46.6 %copy-start.10 = (f32[2048]{0:T(1024)S(1)}, f32[2048]{0:T(1024)}, u32[]{:S(2)}) copy-start(f32[2048]{0:T(1024)} %param.18) | copy-start | bytes 24580
  10.7 46.6 %copy-start.13 = (f32[512]{0:T(512)S(1)}, f32[512]{0:T(512)}, u32[]{:S(2)}) copy-start(f32[512]{0:T(512)} %param.20) | copy-start | bytes 6148
  10.7 198.1 %all-gather.17.cloned.1.call-start = ((), (), s32[]{:S(2)}) async-start(), calls=%async_computation.6 | async-start | bytes 3604480 | tf_op jit(solution)/shard_map/all_gather | solution.py:103
  13.2 90.2 %copy-start.14 = (f32[512]{0:T(512)S(1)}, f32[512]{0:T(512)}, u32[]{:S(2)}) copy-start(f32[512]{0:T(512)} %param.22) | copy-start | bytes 6148
  107.9 41.6 %copy-start.15 = (f32[512]{0:T(512)S(1)}, f32[512]{0:T(512)}, u32[]{:S(2)}) copy-start(f32[512]{0:T(512)} %param.24) | copy-start | bytes 6148
  155.2 5.4 %copy-start.6 = (f32[2,2,2,64,64]{4,3,2,1,0:T(8,128)S(1)}, f32[2,2,2,64,64]{4,3,2,1,0:T(8,128)}, u32[]{:S(2)}) copy-start(f32[2,2,2,64,64]{4,3,2,1,0:T(8,128)} %convolution_multiply_fusion.6) | copy-start | bytes 393220
  163.0 5.1 %copy-start.1 = (bf16[256,2048]{1,0:T(8,128)(2,1)S(1)}, bf16[256,2048]{1,0:T(8,128)(2,1)}, u32[]{:S(2)}) copy-start(bf16[256,2048]{1,0:T(8,128)(2,1)} %param.17) | copy-start | bytes 3145732
  164.6 9.4 %all-to-all-start = ((bf16[4,64,512]{2,1,0:T(8,128)(2,1)}), bf16[4,64,512]{2,1,0:T(8,128)(2,1)S(1)}, u32[]{:S(2)}, u32[]{:S(2)}) async-start(bf16[4,64,512]{2,1,0:T(8,128)(2,1)} %multiply_convert_fusion.2), calls=%async_computation | async-start | bytes 524288 | tf_op jit(solution)/shard_map/all_to_all | solution.py:129
  168.1 57.7 %all-gather.15.cloned.1.call-start = ((), (), s32[]{:S(2)}) async-start(), calls=%async_computation.5 | async-start | bytes 1310720 | tf_op jit(solution)/shard_map/all_gather | solution.py:134
  168.4 6.0 %copy-start.7 = (f32[2048]{0:T(1024)S(1)}, f32[2048]{0:T(1024)}, u32[]{:S(2)}) copy-start(f32[2048]{0:T(1024)} %param.25) | copy-start | bytes 24580
  174.3 3.4 copy-start.3
  175.2 111.1 %all-gather.19.cloned.1.call-start = ((), (), s32[]{:S(2)}) async-start(), calls=%async_computation.7 | async-start | bytes 3604480 | tf_op jit(solution)/shard_map/all_gather | solution.py:104
  177.6 1.1 copy-start.8
  177.6 48.2 %copy-start.11 = (f32[704]{0:T(1024)S(1)}, f32[704]{0:T(1024)}, u32[]{:S(2)}) copy-start(f32[704]{0:T(1024)} %param.27) | copy-start | bytes 8452
  177.6 168.1 %all-gather.21.cloned.1.call-start = ((), (), s32[]{:S(2)}) async-start(), calls=%async_computation.8 | async-start | bytes 3604480 | tf_op jit(solution)/shard_map/all_gather | solution.py:105
  178.6 197.7 %reduce-scatter.2.cloned.1.call-start = ((), (), s32[]{:S(2)}) async-start(), calls=%async_computation.9 | async-start | bytes 1310720 | tf_op jit(solution)/shard_map/reduce_scatter | solution.py:146
  191.3 154.4 %copy-start.12 = (f32[704]{0:T(1024)S(1)}, f32[704]{0:T(1024)}, u32[]{:S(2)}) copy-start(f32[704]{0:T(1024)} %param.29) | copy-start | bytes 8452
  225.8 120.0 %copy-start.9 = (bf16[256,2048]{1,0:T(8,128)(2,1)S(1)}, bf16[256,2048]{1,0:T(8,128)(2,1)}, u32[]{:S(2)}) copy-start(bf16[256,2048]{1,0:T(8,128)(2,1)} %all-gather.15.cloned.1.call-done) | copy-start | bytes 3145732
Sparse Core Ops, SparseCore 0:
  8.9 48.3 all-gather.10
  58.9 44.4 all-gather.12
  105.0 44.4 all-gather.8
  150.9 57.9 all-gather.16
  210.3 15.4 all-gather.14
  227.2 59.1 all-gather.18
  287.9 57.7 all-gather.20
  352.8 23.4 reduce-scatter.1
where the time goes:
time: 385 us
  waiting for transfers between devices  309 us (80%)
  matrix products  26.8 us (7%)
  between operations  13.9 us (4%)
  other arithmetic  13.5 us (4%)
  blocking collectives  12.6 us (3%)
  local copies, waits for them, and re-layouts  5.14 us (1%)
    all_gather x1, waiting for transfers between devices, shards(): lax.all_gather(down_rounded, 'fs', axis=0, tiled=True)  59.4 us
    all_gather x1, waiting for transfers between devices, shards(): lax.all_gather(up_rounded, 'fs', axis=0, tiled=True)  57.4 us
    all_gather x1, waiting for transfers between devices, shards(): lax.all_gather(query_rounded, 'fs', axis=0, tiled=True)  44.2 us
    all_gather x1, waiting for transfers between devices, shards(): lax.all_gather(key_rounded, 'fs', axis=0, tiled=True)  43.4 us
    all_gather x1, waiting for transfers between devices, shards(): lax.all_gather(value_rounded, 'fs', axis=0, tiled=True)  41.1 us
    reduce_scatter x1, waiting for transfers between devices, shards(): lax.psum_scatter(partial_sum.astype(jnp.float32).astype(jnp.bfloat16), 't...  23.6 us
    all_gather x1, waiting for transfers between devices, shards(): lax.all_gather(gate_rounded, 'fs', axis=0, tiled=True)  17.6 us
    all_gather x1, waiting for transfers between devices, shards(): piece = lax.all_gather(normed_ffn, 'tp', axis=0, tiled=True)  16.9 us
  transfers between devices with their start and end apart: 9, of which 9 were waited for; matrix products, arithmetic and copies ran while one was open for 9% of the time, Pallas kernels for 0%

commit v1 on v0

v1 whole, which is shorter than its diff:
```python
import jax
import jax.numpy as jnp
from jax import lax
from jax.sharding import PartitionSpec as P

DK = 256
DV = 256
LEN = 128


EPS = 1e-06
THETA = 10000.0
HIGH = lax.Precision.HIGHEST


def rms_scale(values):
    return lax.rsqrt(jnp.mean(values * values, axis=-1, keepdims=True) + EPS)


def head_scale(values):
    return 1.0 / jnp.maximum(jnp.sqrt(jnp.mean(values * values, axis=-1, keepdims=True)), 1.0)


def rotate(heads_data, positions):
    half = heads_data.shape[-1] // 2
    frequency = THETA ** (-(jnp.arange(half, dtype=jnp.float32) / half))
    angle = positions.astype(jnp.float32)[:, None] * frequency
    cosine = jnp.cos(angle)
    sine = jnp.sin(angle)
    first = heads_data[..., :half]
    second = heads_data[..., half:]
    return jnp.concatenate(
        [first * cosine - second * sine, second * cosine + first * sine], axis=-1
    )


def retention(queries, keys, values, log_decay):
    offsets = jnp.arange(LEN, dtype=jnp.float32)
    distance = offsets[:, None] - offsets[None, :]
    decay = jnp.where(distance >= 0, jnp.exp(log_decay * jnp.maximum(distance, 0.0)), 0.0)
    queries, keys, values = (
        part.reshape(-1, LEN, part.shape[-1]) for part in (queries, keys, values)
    )
    scores = jnp.einsum("sid,sjd->sij", queries, keys, precision=HIGH) * decay
    retained = jnp.einsum("sij,sje->sie", scores, values, precision=HIGH)
    return retained.reshape(-1, values.shape[-1])


def split_rows(weight, mine):
    half = weight.shape[0] // 2
    return lax.dynamic_slice_in_dim(weight, mine * half, half, 0).astype(jnp.bfloat16)


def gathered(weight, mine):
    own = lax.all_gather(split_rows(weight, mine), "fs", axis=0, tiled=True)
    return own, lax.ppermute(own, "rep", [(0, 1), (1, 0)])


def column_halves(rows, shards_count, mine):
    width = rows.shape[1]
    parts = rows.reshape(rows.shape[0], shards_count, 2, width // (2 * shards_count))
    first = parts[:, :, 0].reshape(rows.shape[0], width // 2)
    second = parts[:, :, 1].reshape(rows.shape[0], width // 2)
    return jnp.where(mine == 0, first, second), jnp.where(mine == 0, second, first)


def dot(left, right):
    return jnp.dot(left, right, preferred_element_type=jnp.float32)


def dot_t(left, right):
    return lax.dot_general(left, right, (((1,), (1,)), ((), ())), preferred_element_type=jnp.float32)


def project(halves, weight_halves):
    return dot(halves[0], weight_halves[0]) + dot(halves[1], weight_halves[1])


def shards(
    stream,
    gain_mix,
    w_query,
    scale_query,
    w_key,
    scale_key,
    w_value,
    scale_value,
    gain_ffn,
    w_gate,
    scale_gate,
    w_up,
    scale_up,
    w_down,
    scale_down,
):
    group_rows = stream.shape[0]
    fs_count = lax.axis_size("fs")
    paired = lax.axis_size("rep") == 2
    mine = lax.axis_index("rep")
    stream_f = stream.astype(jnp.float32)
    normed = (stream_f * rms_scale(stream_f) * gain_mix).astype(jnp.bfloat16)
    down_scale = lax.all_gather(scale_down, "fs", axis=0, tiled=True)
    if paired:
        query_w, key_w, value_w, gate_w, up_w, down_w = (
            gathered(w, mine) for w in (w_query, w_key, w_value, w_gate, w_up, w_down)
        )
        spread = lambda rows: column_halves(rows, fs_count, mine)
        times = project
    else:
        query_w, key_w, value_w, gate_w, up_w, down_w = (
            lax.all_gather(w.astype(jnp.bfloat16), "fs", axis=0, tiled=True)
            for w in (w_query, w_key, w_value, w_gate, w_up, w_down)
        )
        spread = lambda rows: rows
        times = dot
    normed = spread(normed)
    query = (times(normed, query_w) * scale_query).astype(jnp.bfloat16)
    key = (times(normed, key_w) * scale_key).astype(jnp.bfloat16)
    value = (times(normed, value_w) * scale_value).astype(jnp.bfloat16)
    local_heads = query.shape[1] // DK
    positions = jnp.arange(group_rows, dtype=jnp.int32) % LEN
    mixed = []
    for head in range(local_heads):
        columns = slice(head * DK, (head + 1) * DK)
        queries = rotate(query[:, columns].astype(jnp.float32), positions)
        keys = rotate(key[:, columns].astype(jnp.float32), positions) * DK ** (-0.5)
        values = value[:, head * DV : (head + 1) * DV].astype(jnp.float32)
        head_id = (lax.axis_index("tp") * local_heads + head).astype(jnp.float32)
        log_decay = jnp.log(1.0 - jnp.power(2.0, -5.0 - head_id))
        retained = retention(queries, keys, values, log_decay)
        mixed.append((retained * head_scale(retained)).astype(jnp.bfloat16))
    mixed = jnp.concatenate(mixed, axis=1)
    arrived = lax.all_to_all(mixed, "tp", split_axis=0, concat_axis=1, tiled=True)
    share = arrived.shape[0]
    own_rows = lax.dynamic_slice_in_dim(stream, lax.axis_index("tp") * share, share, 0)
    resid = own_rows.astype(jnp.float32) + arrived.astype(jnp.float32)
    normed_ffn = (resid * rms_scale(resid) * gain_ffn).astype(jnp.bfloat16)
    piece = spread(lax.all_gather(normed_ffn, "tp", axis=0, tiled=True))
    gate = times(piece, gate_w) * scale_gate
    upward = times(piece, up_w) * scale_up
    hidden = (jax.nn.silu(gate) * upward).astype(jnp.bfloat16)
    if paired:
        own, other = (dot_t(hidden, w).reshape(group_rows, fs_count, 1, -1) for w in down_w)
        first = jnp.where(mine == 0, own, other)
        second = jnp.where(mine == 0, other, own)
        partial_sum = jnp.concatenate([first, second], axis=2).reshape(group_rows, -1)
    else:
        partial_sum = dot_t(hidden, down_w)
    partial_sum = (partial_sum * down_scale).astype(jnp.bfloat16)
    partial_sum = partial_sum.reshape(-1, share, partial_sum.shape[1])
    pieces = lax.all_to_all(partial_sum, "tp", split_axis=0, concat_axis=0)
    channel_out = jnp.sum(pieces.astype(jnp.float32), axis=0)
    return (resid + channel_out).astype(jnp.bfloat16)


def solution(mesh):
    placed = (
        P(("rep", "fs"), None),
        P(),
        P("fs", "tp"),
        P("tp"),
        P("fs", "tp"),
        P("tp"),
        P("fs", "tp"),
        P("tp"),
        P(),
        P("fs", "tp"),
        P("tp"),
        P("fs", "tp"),
        P("tp"),
        P("fs", "tp"),
        P("fs"),
    )
    return jax.shard_map(
        shards, mesh=mesh, in_specs=placed, out_specs=P(("rep", "fs", "tp"), None), check_vma=False
    )
```

time: 385 us -> 279 us (0.72)
  waiting for transfers between devices: 309 us -> 171 us
  local copies, waits for them, and re-layouts: 5.14 us -> 22.7 us
  blocking collectives: 12.6 us -> 29.6 us
  matrix products: 26.8 us -> 15.5 us
  starting transfers between devices: 3.7 us -> 12.6 us
    all_gather x7, waiting for transfers between devices: 280 us -> 141 us  [the longest x6 126 us: gathered(): own = lax.all_gather(split_rows(weight, mine), 'fs', axis=0, tiled=True)]
    ppermute x0 -> x6, waiting for transfers between devices: none -> 24.2 us  [gathered(): return (own, lax.ppermute(own, 'rep', [(0, 1), (1, 0)]))]
    reduce_scatter x1 -> x0, waiting for transfers between devices: 23.6 us -> none  [shards(): lax.psum_scatter(partial_sum.astype(jnp.float32).astype(jnp.bfloat16), 't...]
    all_to_all x0 -> x1, blocking collectives: none -> 17.4 us  [shards(): pieces = lax.all_to_all(partial_sum, 'tp', split_axis=0, concat_axis=0)]
    dot_general x11 -> x16, matrix products: 26.8 us -> 15.5 us  [the longest x10 11.5 us: dot(): return jnp.dot(left, right, preferred_element_type=jnp.float32)]
    convert_element_type x1 -> x7, local copies, waits for them, and re-layouts: 0.04 us -> 10.2 us  [the longest x6 10.1 us: split_rows(): lax.dynamic_slice_in_dim(weight, mine * half, half, 0).astype(jnp.bfloat16)]
    ppermute x0 -> x6, starting transfers between devices: none -> 8.9 us  [gathered(): return (own, lax.ppermute(own, 'rep', [(0, 1), (1, 0)]))]
    convert_element_type x9 -> x7, other arithmetic: 9.26 us -> 2.4 us  [the longest x1 1.77 us: shards(): partial_sum = (partial_sum * down_scale).astype(jnp.bfloat16)]
  transfers between devices with their start and end apart: 9 -> 14, of which waited for: 9 -> 9; matrix products, arithmetic and copies ran while one was open for 9% -> 11% of each run, Pallas kernels for 0% -> 0%
where the time goes in v1:
time: 279 us; the launch traced here: 278 us
  waiting for transfers between devices  171 us (61%)
  blocking collectives  29.6 us (11%)
  local copies, waits for them, and re-layouts  22.7 us (8%)
  matrix products  15.5 us (6%)
  between operations  14.2 us (5%)
  starting transfers between devices  12.6 us (5%)
  other arithmetic  12.5 us (4%)
    all_gather x6, waiting for transfers between devices, gathered(): own = lax.all_gather(split_rows(weight, mine), 'fs', axis=0, tiled=True)  126 us
    ppermute x6, waiting for transfers between devices, gathered(): return (own, lax.ppermute(own, 'rep', [(0, 1), (1, 0)]))  24.2 us
    all_to_all x1, blocking collectives, shards(): pieces = lax.all_to_all(partial_sum, 'tp', split_axis=0, concat_axis=0)  17.4 us
    all_gather x1, waiting for transfers between devices, shards(): piece = spread(lax.all_gather(normed_ffn, 'tp', axis=0, tiled=True))  15 us
    all_gather x1, blocking collectives, shards(): down_scale = lax.all_gather(scale_down, 'fs', axis=0, tiled=True)  12.3 us
    dot_general x10, matrix products, dot(): return jnp.dot(left, right, preferred_element_type=jnp.float32)  11.5 us
    convert_element_type x6, local copies, waits for them, and re-layouts, split_rows(): lax.dynamic_slice_in_dim(weight, mine * half, half, 0).astype(jnp.bfloat16)  10.1 us
    ppermute x6, starting transfers between devices, gathered(): return (own, lax.ppermute(own, 'rep', [(0, 1), (1, 0)]))  8.9 us
  transfers between devices with their start and end apart: 14, of which 9 were waited for; matrix products, arithmetic and copies ran while one was open for 11% of the time, Pallas kernels for 0%

profile of v1, /device:TPU:0, one launch (start us, length us, event | category | flops | bytes accessed | tf_op | source)
XLA Modules:
  0.0 278.4 jit_solution(3563157175926531187)
XLA Ops:
  6.5 1.9 dynamic-slice_convert_fusion.5
  8.6 1.8 dynamic-slice_convert_fusion.4
  10.4 1.8 dynamic-slice_convert_fusion.3
  13.1 2.0 dynamic-slice_convert_fusion.1
  15.2 1.9 dynamic-slice_convert_fusion
  20.3 19.3 %all-gather.9.cloned.1.call-done = bf16[1024,512]{1,0:T(8,128)(2,1)} async-done(((bf16[256,512]{1,0:T(8,128)(2,1)}), bf16[1024,512]{1,0:T(8,128)(2,1)}) %all-gather.9.cloned.1.call-update) | async-done | bytes 1048592 | tf_op jit(solution)/shard_map/all_gather | solution.py:55
  41.2 27.4 %all-gather.11.cloned.1.call-done = bf16[1024,512]{1,0:T(8,128)(2,1)} async-done(((bf16[256,512]{1,0:T(8,128)(2,1)}), bf16[1024,512]{1,0:T(8,128)(2,1)}) %all-gather.11.cloned.1.call-update) | async-done | bytes 1048592 | tf_op jit(solution)/shard_map/all_gather | solution.py:55
  70.1 27.5 %all-gather.13.cloned.1.call-done = bf16[1024,512]{1,0:T(8,128)(2,1)} async-done(((bf16[256,512]{1,0:T(8,128)(2,1)}), bf16[1024,512]{1,0:T(8,128)(2,1)}) %all-gather.13.cloned.1.call-update) | async-done | bytes 1048592 | tf_op jit(solution)/shard_map/all_gather | solution.py:55
  97.6 1.5 collective-permute-start.2
  99.0 1.7 fusion.49
  102.6 1.7 fusion.10
  104.4 1.7 fusion.9
  106.2 16.0 %collective-permute-done.2 = bf16[1024,512]{1,0:T(8,128)(2,1)S(1)} collective-permute-done((bf16[1024,512]{1,0:T(8,128)(2,1)}, bf16[1024,512]{1,0:T(8,128)(2,1)S(1)}, u32[]{:S(2)}, u32[]{:S(2)}) %collective-permute-start.2) | collective-permute-done | bytes 1048608 | tf_op jit(solution)/shard_map/ppermute | solution.py:56
  126.2 3.4 %all-to-all-start = ((bf16[4,64,512]{2,1,0:T(8,128)(2,1)}), bf16[4,64,512]{2,1,0:T(8,128)(2,1)S(1)}, u32[]{:S(2)}, u32[]{:S(2)}) async-start(bf16[4,64,512]{2,1,0:T(8,128)(2,1)} %pad_maximum_fusion.3), calls=%async_computation | async-start | bytes 524288 | tf_op jit(solution)/shard_map/all_to_all | solution.py:133
  129.7 5.9 %all-to-all-done = bf16[4,64,512]{2,1,0:T(8,128)(2,1)S(1)} async-done(((bf16[4,64,512]{2,1,0:T(8,128)(2,1)}), bf16[4,64,512]{2,1,0:T(8,128)(2,1)S(1)}, u32[]{:S(2)}, u32[]{:S(2)}) %all-to-all-start) | async-done | bytes 262176 | tf_op jit(solution)/shard_map/all_to_all | solution.py:133
  137.4 1.5 collective-permute-start.3
  138.9 30.3 %all-gather.19.cloned.1.call-done = bf16[1024,704]{0,1:T(8,128)(2,1)} async-done(((bf16[256,704]{0,1:T(8,128)(2,1)}), bf16[1024,704]{0,1:T(8,128)(2,1)}) %all-gather.19.cloned.1.call-update) | async-done | bytes 1441808 | tf_op jit(solution)/shard_map/all_gather | solution.py:55
  170.7 12.3 %all-gather = f32[4,1,512]{2,1,0:T(1,128)S(1)} all-gather(f32[1,1,512]{2,1,0:T(1,128)S(1)} %bitcast.78), channel_id=1, replica_groups=mesh['rep'=2,'fs'=4,'tp'=4] {'fs'}, dimensions={0}, use_global_device_ids=true | all-gather | bytes 10240 | tf_op jit(solution)/shard_map/all_gather | solution.py:102
  182.9 21.5 %all-gather.21.cloned.1.call-done = bf16[1024,704]{0,1:T(8,128)(2,1)} async-done(((bf16[256,704]{0,1:T(8,128)(2,1)}), bf16[1024,704]{0,1:T(8,128)(2,1)}) %all-gather.21.cloned.1.call-update) | async-done | bytes 1441808 | tf_op jit(solution)/shard_map/all_gather | solution.py:55
  205.9 15.0 %all-gather.15.cloned.1.call-done = bf16[256,2048]{1,0:T(8,128)(2,1)} async-done(((bf16[64,2048]{1,0:T(8,128)(2,1)}), bf16[256,2048]{1,0:T(8,128)(2,1)}) %all-gather.15.cloned.1.call-update) | async-done | bytes 1048592 | tf_op jit(solution)/shard_map/all_gather | solution.py:138
  220.9 1.5 copy.28
  225.0 1.9 fusion.4
  227.0 2.0 multiply_convert_fusion.1
  229.6 8.2 %collective-permute-done.5 = bf16[1024,704]{0,1:T(8,128)(2,1)} collective-permute-done((bf16[1024,704]{0,1:T(8,128)(2,1)}, bf16[1024,704]{0,1:T(8,128)(2,1)}, u32[]{:S(2)}, u32[]{:S(2)}) %collective-permute-start.5) | collective-permute-done | bytes 1441824 | tf_op jit(solution)/shard_map/ppermute | solution.py:56
  237.9 2.0 broadcast_select_fusion.1
  239.8 2.2 select_n.152
  242.1 2.2 select_n.153
  244.3 3.4 %pad_maximum_fusion = f32[256,4,2,256]{3,2,1,0:T(2,128)S(1)} fusion(f32[256,4,1,256]{3,2,1,0:T(1,128)} %select_n.153, f32[256,4,1,256]{3,2,1,0:T(1,128)} %select_n.152), kind=kLoop, calls=%fused_computation.5 | loop fusion | flops 524288 | bytes 4194304 | tf_op jit(solution)/shard_map/concatenate | solution.py:146
  247.8 2.7 reshape.232
  250.4 1.8 multiply_convert_fusion
  252.2 17.4 %all_to_all.15 = bf16[4,64,2048]{2,1,0:T(8,128)(2,1)S(1)} all-to-all(bf16[4,64,2048]{2,1,0:T(8,128)(2,1)S(1)} %multiply_convert_fusion), channel_id=1, replica_groups=mesh['rep'=2,'fs'=4,'tp'=4] {'tp'}, dimensions={0} | all-to-all | bytes 2097152 | tf_op jit(solution)/shard_map/all_to_all | solution.py:151
  269.8 1.7 add_convert_fusion
  (104 shorter events, 21.1 us)
Async XLA Ops:
  6.5 5.7 %copy-start = (f32[512,704]{0,1:T(8,128)S(1)}, f32[512,704]{0,1:T(8,128)}, u32[]{:S(2)}) copy-start(f32[512,704]{0,1:T(8,128)} %param.24) | copy-start | bytes 4325380
  6.5 33.1 %all-gather.9.cloned.1.call-start = ((), (), s32[]{:S(2)}) async-start(), calls=%async_computation.2 | async-start | bytes 1310720 | tf_op jit(solution)/shard_map/all_gather | solution.py:55
  8.5 60.1 %all-gather.11.cloned.1.call-start = ((), (), s32[]{:S(2)}) async-start(), calls=%async_computation.3 | async-start | bytes 1310720 | tf_op jit(solution)/shard_map/all_gather | solution.py:55
  10.4 87.2 %all-gather.13.cloned.1.call-start = ((), (), s32[]{:S(2)}) async-start(), calls=%async_computation.4 | async-start | bytes 1310720 | tf_op jit(solution)/shard_map/all_gather | solution.py:55
  12.2 125.2 %all-gather.17.cloned.1.call-start = ((), (), s32[]{:S(2)}) async-start(), calls=%async_computation.6 | async-start | bytes 1802240 | tf_op jit(solution)/shard_map/all_gather | solution.py:55
  13.1 4.6 %copy-start.3 = (bf16[256,2048]{1,0:T(8,128)(2,1)S(1)}, bf16[256,2048]{1,0:T(8,128)(2,1)}, u32[]{:S(2)}) copy-start(bf16[256,2048]{1,0:T(8,128)(2,1)} %param.15) | copy-start | bytes 3145732
  13.1 156.1 %all-gather.19.cloned.1.call-start = ((), (), s32[]{:S(2)}) async-start(), calls=%async_computation.7 | async-start | bytes 1802240 | tf_op jit(solution)/shard_map/all_gather | solution.py:55
  15.1 189.3 %all-gather.21.cloned.1.call-start = ((), (), s32[]{:S(2)}) async-start(), calls=%async_computation.8 | async-start | bytes 1802240 | tf_op jit(solution)/shard_map/all_gather | solution.py:55
  17.6 2.3 copy-start.12
  39.6 62.8 %collective-permute-start = (bf16[1024,512]{1,0:T(8,128)(2,1)}, bf16[1024,512]{1,0:T(8,128)(2,1)}, u32[]{:S(2)}, u32[]{:S(2)}) collective-permute-start(bf16[1024,512]{1,0:T(8,128)(2,1)} %all-gather.9.cloned.1.call-done), channel_id=1, source_target_pairs={{0,16},{16,0},{1,17},{17,1},{2,18},{18,2},{3,19},{19,3},{4,20},{20... | collective-permute-start | bytes 3145736 | tf_op jit(solution)/shard_map/ppermute | solution.py:56
  68.6 32.1 %copy-start.8 = (bf16[1024,512]{1,0:T(8,128)(2,1)S(1)}, bf16[1024,512]{1,0:T(8,128)(2,1)}, u32[]{:S(2)}) copy-start(bf16[1024,512]{1,0:T(8,128)(2,1)} %all-gather.11.cloned.1.call-done) | copy-start | bytes 3145732
  68.6 35.8 %collective-permute-start.1 = (bf16[1024,512]{1,0:T(8,128)(2,1)}, bf16[1024,512]{1,0:T(8,128)(2,1)}, u32[]{:S(2)}, u32[]{:S(2)}) collective-permute-start(bf16[1024,512]{1,0:T(8,128)(2,1)} %all-gather.11.cloned.1.call-done), channel_id=1, source_target_pairs={{0,16},{16,0},{1,17},{17,1},{2,18},{18,2},{3,19},{19,3},{4,20},{20... | collective-permute-start | bytes 3145736 | tf_op jit(solution)/shard_map/ppermute | solution.py:56
  97.6 24.6 %collective-permute-start.2 = (bf16[1024,512]{1,0:T(8,128)(2,1)}, bf16[1024,512]{1,0:T(8,128)(2,1)S(1)}, u32[]{:S(2)}, u32[]{:S(2)}) collective-permute-start(bf16[1024,512]{1,0:T(8,128)(2,1)} %all-gather.13.cloned.1.call-done), channel_id=1, source_target_pairs={{0,16},{16,0},{1,17},{17,1},{2,18},{18,2},{3,19},{19,3},{4,20},{20... | collective-permute-start | bytes 3145736 | tf_op jit(solution)/shard_map/ppermute | solution.py:56
  100.7 1.2 copy-start.9
  102.6 1.8 copy-start.17
  104.4 17.8 %copy-start.18 = (f32[512]{0:T(512)S(1)}, f32[512]{0:T(512)}, u32[]{:S(2)}) copy-start(f32[512]{0:T(512)} %param.22) | copy-start | bytes 6148
  106.2 16.5 %copy-start.19 = (f32[128]{0:T(128)S(1)}, f32[128]{0:T(128)}, u32[]{:S(2)}) copy-start(f32[128]{0:T(128)} %negate_power_fusion) | copy-start | bytes 1540
  122.7 0.8 copy-start.10
  123.4 0.9 copy-start.11
  125.5 10.2 %copy-start.4 = (bf16[256,2048]{1,0:T(8,128)(2,1)S(1)}, bf16[256,2048]{1,0:T(8,128)(2,1)}, u32[]{:S(2)}) copy-start(bf16[256,2048]{1,0:T(8,128)(2,1)} %param.15) | copy-start | bytes 3145732
  126.2 9.4 %all-to-all-start = ((bf16[4,64,512]{2,1,0:T(8,128)(2,1)}), bf16[4,64,512]{2,1,0:T(8,128)(2,1)S(1)}, u32[]{:S(2)}, u32[]{:S(2)}) async-start(bf16[4,64,512]{2,1,0:T(8,128)(2,1)} %pad_maximum_fusion.3), calls=%async_computation | async-start | bytes 524288 | tf_op jit(solution)/shard_map/all_to_all | solution.py:133
  129.6 6.9 %copy-start.13 = (f32[2048]{0:T(1024)S(1)}, f32[2048]{0:T(1024)}, u32[]{:S(2)}) copy-start(f32[2048]{0:T(1024)} %param.23) | copy-start | bytes 24580
  129.6 91.3 %all-gather.15.cloned.1.call-start = ((), (), s32[]{:S(2)}) async-start(), calls=%async_computation.5 | async-start | bytes 1310720 | tf_op jit(solution)/shard_map/all_gather | solution.py:138
  135.7 35.0 %copy-start.15 = (f32[512]{0:T(512)S(1)}, f32[512]{0:T(512)}, u32[]{:S(2)}) copy-start(f32[512]{0:T(512)} %param.29) | copy-start | bytes 6148
  137.4 87.5 %collective-permute-start.3 = (bf16[1024,704]{0,1:T(8,128)(2,1)}, bf16[1024,704]{0,1:T(8,128)(2,1)}, u32[]{:S(2)}, u32[]{:S(2)}) collective-permute-start(bf16[1024,704]{0,1:T(8,128)(2,1)} %all-gather.17.cloned.1.call-done), channel_id=1, source_target_pairs={{0,16},{16,0},{1,17},{17,1},{2,18},{18,2},{3,19},{19,3},{4,20},{20... | collective-permute-start | bytes 4325384 | tf_op jit(solution)/shard_map/ppermute | solution.py:56
  169.2 57.8 %collective-permute-start.4 = (bf16[1024,704]{0,1:T(8,128)(2,1)}, bf16[1024,704]{0,1:T(8,128)(2,1)}, u32[]{:S(2)}, u32[]{:S(2)}) collective-permute-start(bf16[1024,704]{0,1:T(8,128)(2,1)} %all-gather.19.cloned.1.call-done), channel_id=1, source_target_pairs={{0,16},{16,0},{1,17},{17,1},{2,18},{18,2},{3,19},{19,3},{4,20},{20... | collective-permute-start | bytes 4325384 | tf_op jit(solution)/shard_map/ppermute | solution.py:56
  204.5 33.4 %collective-permute-start.5 = (bf16[1024,704]{0,1:T(8,128)(2,1)}, bf16[1024,704]{0,1:T(8,128)(2,1)}, u32[]{:S(2)}, u32[]{:S(2)}) collective-permute-start(bf16[1024,704]{0,1:T(8,128)(2,1)} %all-gather.21.cloned.1.call-done), channel_id=1, source_target_pairs={{0,16},{16,0},{1,17},{17,1},{2,18},{18,2},{3,19},{19,3},{4,20},{20... | collective-permute-start | bytes 4325384 | tf_op jit(solution)/shard_map/ppermute | solution.py:56
  222.4 1.4 copy-start.6
  222.5 1.8 copy-start.7
  225.0 1.9 copy-start.20
  226.9 2.1 copy-start.5
  252.2 17.5 %copy-start.2 = (f32[4,8,8,512]{3,2,0,1:T(8,128)S(1)}, f32[4,8,8,512]{3,2,0,1:T(8,128)}, u32[]{:S(2)}) copy-start(f32[4,8,8,512]{3,2,0,1:T(8,128)} %copy-done.1) | copy-start | bytes 1572868
  (3 other events, 2.2 us)
Sparse Core Ops, SparseCore 0:
  8.9 30.6 all-gather.8
  41.2 27.3 all-gather.10
  70.2 27.3 all-gather.12
  99.0 34.9 all-gather.16
  135.4 33.7 all-gather.18
  170.6 33.7 all-gather.20
  206.0 14.8 all-gather.14
